TPU v7x, 32 devices: a whole 2x2x4 slice. The times are simulated.
32 devices in a mesh: ep: 8 (over z, x), tp: 4 (over y, core).
Axes of the slice: x: 2, y: 2, z: 4, core: 2. Of those that a mesh axis runs over, the one named last changes fastest.
Arguments:
- queries: bfloat16 [2048, 2, 1024], P('ep', None, 'tp')
- keys: bfloat16 [2048, 2, 256], P('ep', None, 'tp')
- values: bfloat16 [2048, 2, 256], P('ep', None, 'tp'), may hold values from -6 to 6
- query_gain: float32 [64], replicated, may hold values from 1.2 to 6
- key_gain: float32 [64], replicated, may hold values from 1.2 to 6
- out_weight: bfloat16 [1024, 2048], P('tp'), may hold values from -0.75 to 0.75
- moe_tokens: bfloat16 [4096, 2048], P(('ep', 'tp')), may hold values from -6 to 6
- moe_gain: float32 [2048], replicated, may hold values from 0.1 to 1.9
- routes: int32 [4096, 2], P(('ep', 'tp')), may hold values from 0 to 7, all different within a row; in each aligned block of 128 rows (0 to 127, 128 to 255, ...) at most 48 rows name the same one
- route_weight: float32 [4096, 2], P(('ep', 'tp')), may hold values from 0.1 to 1
- w_gate: bfloat16 [8, 2048, 1024], P('ep', None, 'tp'), may hold values from -0.125 to 0.125
- w_up: bfloat16 [8, 2048, 1024], P('ep', None, 'tp'), may hold values from -0.125 to 0.125
- w_down: bfloat16 [8, 1024, 2048], P('ep', 'tp'), may hold values from -0.1875 to 0.1875
Outputs:
- attended: bfloat16 [2048, 2, 2048], P(('ep', 'tp'))
- routed: bfloat16 [4096, 2048], P(('ep', 'tp'))
Inputs may be any that keep to these rules, and one draw needn't show every extreme that they name: `routes`: each row names 2 different experts. The rows of one device name no expert more than 48 times, and in every draw some device's rows name one expert exactly 48 times.
All inputs are finite; a program needn't handle non-finite values.
Results may differ from a plain program's by a relative error of at most 0.013.
The roundings to bfloat16 on the way count: a program that leaves them out, or rounds other values in their place, can miss the bound.
Values may be sent and summed in bfloat16 or wider, within the bound.
A program may use at most 128 MiB of HBM per device.

v0:
```python
import math
import jax
import jax.numpy as jnp
from jax import lax
from jax.sharding import PartitionSpec as P

HEAD_DIM = 64
GRID_W = 64
EPS = 1e-06
THETA = 10000.0


def turn(normed, positions):
    quarter = normed.shape[-1] // 4
    inverse = THETA ** (-jnp.arange(quarter, dtype=jnp.float32) / quarter)
    grid_row = (positions // GRID_W).astype(jnp.float32)
    grid_col = (positions % GRID_W).astype(jnp.float32)
    angles = jnp.stack([grid_row[:, None] * inverse, grid_col[:, None] * inverse], axis=1)
    cosine = jnp.cos(angles)[:, None, None]
    sine = jnp.sin(angles)[:, None, None]
    parts = normed.reshape(normed.shape[:-1] + (2, 2, quarter))
    first = parts[..., 0, :]
    second = parts[..., 1, :]
    turned = jnp.stack([first * cosine - second * sine, second * cosine + first * sine], axis=-2)
    return turned.reshape(normed.shape)


def prepare(data, positions, gain):
    heads = data.astype(jnp.float32).reshape(data.shape[0], data.shape[1], -1, HEAD_DIM)
    normed = heads * lax.rsqrt(jnp.mean(heads * heads, axis=-1, keepdims=True) + EPS) * gain
    return turn(normed, positions).astype(jnp.bfloat16)


def per_device(
    queries,
    keys,
    values,
    query_gain,
    key_gain,
    out_weight,
    moe_tokens,
    moe_gain,
    routes,
    route_weight,
    w_gate,
    w_up,
    w_down,
):
    pos_count = queries.shape[0]
    seq_count = queries.shape[1]
    positions = lax.axis_index("ep") * pos_count + jnp.arange(pos_count, dtype=jnp.int32)
    q_rot = prepare(queries, positions, query_gain)
    k_rot = prepare(keys, positions, key_gain)
    kv_local = k_rot.shape[2]
    groups = q_rot.shape[2] // kv_local
    value_heads = values.reshape(pos_count, seq_count, kv_local, HEAD_DIM)
    q_group = q_rot.reshape(pos_count, seq_count, kv_local, groups, HEAD_DIM)
    scale = HEAD_DIM ** (-0.5)
    start_state = (
        jnp.full((seq_count, kv_local, groups, pos_count), -1e30, jnp.float32),
        jnp.zeros((seq_count, kv_local, groups, pos_count), jnp.float32),
        jnp.zeros((pos_count, seq_count, kv_local, groups, HEAD_DIM), jnp.float32),
    )
    carry = start_state
    key_piece = lax.all_gather(k_rot, "ep", axis=0, tiled=True)
    value_piece = lax.all_gather(value_heads, "ep", axis=0, tiled=True)
    count = key_piece.shape[0]
    width = math.gcd(count, 512)
    key_split = key_piece.reshape(count // width, width, seq_count, kv_local, HEAD_DIM)
    value_split = value_piece.reshape(count // width, width, seq_count, kv_local, HEAD_DIM)

    def step(state, block):
        best, total, accum = state
        key_block, value_block = block
        scores = (
            jnp.einsum("pskgd,lskd->skgpl", q_group, key_block, preferred_element_type=jnp.float32)
            * scale
        )
        new_best = jnp.maximum(best, jnp.max(scores, axis=-1))
        factor = jnp.exp(best - new_best)
        expo = jnp.exp(scores - new_best[..., None])
        total = total * factor + jnp.sum(expo, axis=-1)
        added = jnp.einsum(
            "skgpl,lskd->pskgd",
            expo.astype(jnp.bfloat16),
            value_block,
            preferred_element_type=jnp.float32,
        )
        accum = accum * jnp.transpose(factor, (3, 0, 1, 2))[..., None] + added
        return ((new_best, total, accum), None)

    carry, _ = lax.scan(step, carry, (key_split, value_split))
    best, total, accum = carry
    mixed = (accum / jnp.transpose(total, (3, 0, 1, 2))[..., None]).astype(jnp.bfloat16)
    mixed = mixed.reshape(pos_count, seq_count, -1)
    rows = mixed
    product = jnp.dot(
        rows.reshape(pos_count // lax.axis_size("tp") * lax.axis_size("tp") * seq_count, -1),
        out_weight,
        preferred_element_type=jnp.float32,
    )
    attended = lax.psum_scatter(
        product.reshape(
            pos_count // lax.axis_size("tp") * lax.axis_size("tp"), seq_count, -1
        ).astype(jnp.bfloat16),
        "tp",
        scatter_dimension=0,
        tiled=True,
    )
    tok_count = moe_tokens.shape[0]
    top_count = routes.shape[1]
    experts = lax.axis_size("ep")
    capacity = max(2, (3 * tok_count * top_count + 2 * experts - 1) // (2 * experts))
    token_float = moe_tokens.astype(jnp.float32)
    normed = (
        token_float
        * lax.rsqrt(jnp.mean(token_float * token_float, axis=-1, keepdims=True) + EPS)
        * moe_gain
    ).astype(jnp.bfloat16)
    hits = (routes[:, :, None] == jnp.arange(experts, dtype=jnp.int32)[None, None, :]).astype(
        jnp.float32
    )
    pair_count = tok_count * top_count
    flat_hits = hits.reshape(pair_count, experts)
    pair_index = jnp.arange(pair_count, dtype=jnp.int32)
    earlier = (pair_index[:, None] > pair_index[None, :]).astype(jnp.float32)
    before = jnp.dot(earlier, flat_hits, precision=lax.Precision.HIGHEST)
    rank = jnp.sum(before * flat_hits, axis=-1).astype(jnp.int32).reshape(tok_count, top_count)
    slot = routes * capacity + rank
    table = jnp.arange(experts * capacity, dtype=jnp.int32)
    dispatch = jnp.sum(
        (slot[None, :, :] == table[:, None, None]).astype(jnp.float32), axis=2
    ).astype(jnp.bfloat16)
    send = jnp.dot(dispatch, normed, preferred_element_type=jnp.float32).astype(jnp.bfloat16)
    received = lax.all_to_all(send, "ep", split_axis=0, concat_axis=0, tiled=True)
    rows = lax.all_gather(received, "tp", axis=0, tiled=True)
    gate = jnp.dot(rows, w_gate[0], preferred_element_type=jnp.float32)
    up = jnp.dot(rows, w_up[0], preferred_element_type=jnp.float32)
    hidden = (jax.nn.silu(gate) * up).astype(jnp.bfloat16)
    rows = hidden
    result = lax.psum_scatter(
        jnp.dot(rows, w_down[0], preferred_element_type=jnp.float32).astype(jnp.bfloat16),
        "tp",
        scatter_dimension=0,
        tiled=True,
    )
    returned_rows = lax.all_to_all(result, "ep", split_axis=0, concat_axis=0, tiled=True)
    combined = jnp.zeros((tok_count, returned_rows.shape[-1]), jnp.float32)
    for choice_index in range(top_count):
        picker = (slot[:, choice_index : choice_index + 1] == table[None, :]).astype(jnp.bfloat16)
        picked = jnp.dot(picker, returned_rows, preferred_element_type=jnp.float32)
        combined = combined + picked * route_weight[:, choice_index : choice_index + 1]
    return (attended, combined.astype(jnp.bfloat16))


def solution(mesh):
    in_specs = (
        P("ep", None, "tp"),
        P("ep", None, "tp"),
        P("ep", None, "tp"),
        P(),
        P(),
        P("tp", None),
        P(("ep", "tp"), None),
        P(),
        P(("ep", "tp"), None),
        P(("ep", "tp"), None),
        P("ep", None, "tp"),
        P("ep", None, "tp"),
        P("ep", "tp", None),
    )
    out_specs = (P(("ep", "tp"), None, None), P(("ep", "tp"), None))
    return jax.shard_map(
        per_device, mesh=mesh, in_specs=in_specs, out_specs=out_specs, check_vma=False
    )
```

profile of v0, /device:TPU:0, one launch (start us, length us, event | category | flops | bytes accessed | tf_op | source)
XLA Modules:
  0.0 241.3 jit_solution(14699746552922616163)
XLA Ops:
  7.2 0.0 copy-start
  7.2 0.0 copy-start.7
  7.2 0.0 all-gather.3.cloned.1.call-start
  7.2 1.4 fusion.28
  8.6 0.8 copy.53
  9.4 0.1 eq.63
  9.5 0.2 fusion.27
  9.8 0.1 convert_element_type.99
  9.9 0.1 copy.54
  10.0 0.7 multiply_add_fusion
  10.7 0.1 convert_reduce_fusion
  10.7 1.7 convolution_convert_fusion.2
  12.4 44.2 %all_to_all.24 = bf16[8,48,2048]{2,1,0:T(8,128)(2,1)} all-to-all(bf16[8,48,2048]{2,1,0:T(8,128)(2,1)S(1)} %bitcast.136), channel_id=1, replica_groups=mesh['ep'=8,'tp'=4] {'ep'}, dimensions={0} | all-to-all | bytes 3145728 | tf_op jit(solution)/shard_map/all_to_all | solution.py:135
  56.6 0.0 all-gather.3.cloned.1.call-update
  56.6 0.0 copy-start.8
  56.7 0.0 reduce-scatter.5.cloned.1.call-start
  56.7 45.5 %all-gather.3.cloned.1.call-done = bf16[1536,2048]{1,0:T(8,128)(2,1)} async-done(((bf16[384,2048]{1,0:T(8,128)(2,1)}), bf16[1536,2048]{1,0:T(8,128)(2,1)}) %all-gather.3.cloned.1.call-update) | async-done | bytes 6291472 | tf_op jit(solution)/shard_map/all_gather | solution.py:136
  102.2 0.0 copy-done.7
  102.2 5.8 %fusion.34 = f32[1536,256]{1,0:T(8,128)} fusion(bf16[1536,2048]{1,0:T(8,128)(2,1)} %all-gather.3.cloned.1.call-done, bf16[1,2048,256]{2,1,0:T(8,128)(2,1)S(1)} %copy-done.7), kind=kOutput, calls=%fused_computation.44 | convolution fusion | flops 1610612736 | bytes 8912896 | tf_op jit(solution)/shard_map/dot_general | solution.py:137
  108.0 0.0 copy-done
  108.0 0.0 copy-done.8
  108.0 12.3 %convolution_convert_fusion = bf16[1536,2048]{1,0:T(8,128)(2,1)} fusion(bf16[1536,2048]{1,0:T(8,128)(2,1)} %all-gather.3.cloned.1.call-done, f32[1536,256]{1,0:T(8,128)} %fusion.34, bf16[1,256,2048]{2,1,0:T(8,128)(2,1)S(1)} %copy-done, bf16[1,2048,256]{2,1,0:T(8,128)(2,1)S(1)} %copy-done.8), kind=kOutput, calls=%fused_computation.26 | convolution fusion | flops 3226730496 | bytes 16252928 | tf_op jit(solution)/shard_map/dot_general | solution.py:142
  120.3 0.0 copy-start.3
  120.3 0.0 reduce-scatter.5.cloned.1.call-update
  120.3 0.0 reduce-scatter.3.cloned.1.call-start
  120.4 0.5 copy-done.6
  120.9 0.1 mul.275
  121.0 0.2 copy-done.2
  121.3 0.2 copy.49
  121.5 0.1 broadcast_multiply_fusion.1
  121.5 0.1 fusion.47
  121.7 0.1 fusion.42
  121.9 31.5 %all_gather.9 = bf16[2048,2,1,64]{0,3,1,2:T(8,128)(2,1)S(1)} all-gather(bf16[256,2,1,64]{0,3,1,2:T(8,128)(2,1)S(1)} %bitcast.146), channel_id=1, replica_groups=mesh['ep'=8,'tp'=4] {'ep'}, dimensions={0}, use_global_device_ids=true | all-gather | bytes 589824 | tf_op jit(solution)/shard_map/all_gather | solution.py:65
  153.4 0.0 copy-done.3
  153.4 31.5 %all-gather = bf16[2048,2,64]{0,2,1:T(8,128)(2,1)S(1)} all-gather(bf16[256,2,64]{0,2,1:T(8,128)(2,1)S(1)} %copy-done.3), channel_id=2, replica_groups=mesh['ep'=8,'tp'=4] {'ep'}, dimensions={0}, use_global_device_ids=true | all-gather | bytes 589824 | tf_op jit(solution)/shard_map/all_gather | solution.py:66
  184.9 0.4 reshape.289
  185.2 0.1 copy.51
  185.3 0.1 bitcast_reduce_fusion.1
  185.4 0.1 multiply_multiply_fusion
  185.5 0.1 subtract_convert_fusion
  185.7 10.0 %while.15 = (s32[]{:T(128)}, f32[2,1,4,256]{3,2,0,1:T(4,128)S(1)}, f32[2,1,4,256]{3,2,0,1:T(4,128)S(1)}, f32[256,2,1,4,64]{0,4,3,1,2:T(8,128)S(1)}, bf16[4,512,2...) while((s32[]{:T(128)}, f32[2,1,4,256]{3,2,0,1:T(4,128)S(1)}, ...), condition=%wide.region_5.6_spmd.clone, body=%wide.region_2.5_spmd.clone.sunk | while | flops 277229568 | bytes 14286969 | solution.py:92
  185.7 0.8 bitcast_reduce_fusion.3
  186.5 0.7 fusion.67
  187.2 0.9 fusion.68
  188.2 0.8 bitcast_reduce_fusion.3
  189.0 0.7 fusion.67
  189.7 0.9 fusion.68
  190.7 0.8 bitcast_reduce_fusion.3
  191.5 0.7 fusion.67
  192.2 0.9 fusion.68
  193.2 0.8 bitcast_reduce_fusion.3
  194.0 0.7 fusion.67
  194.7 0.9 fusion.68
  195.7 0.0 copy-start.4
  195.8 3.3 %convolution_convert_fusion.1 = bf16[256,2,2048]{2,0,1:T(8,128)(2,1)} fusion(bf16[256,2,256]{0,2,1:T(8,128)(2,1)S(1)} %bitcast.143, bf16[256,2048]{1,0:T(8,128)(2,1)} %param.20), kind=kOutput, calls=%fused_computation.27 | convolution fusion | flops 537919488 | bytes 3407872 | tf_op jit(solution)/shard_map/dot_general | solution.py:97
  199.1 0.0 reduce-scatter.3.cloned.1.call-update
  199.1 0.0 reduce-scatter.5.cloned.1.call-done
  199.1 5.7 %all-to-all-start.1 = ((bf16[8,48,2048]{2,1,0:T(8,128)(2,1)}), bf16[8,48,2048]{2,1,0:T(8,128)(2,1)S(1)}, u32[]{:S(2)}, u32[]{:S(2)}) async-start(bf16[8,48,2048]{2,1,0:T(8,128)(2,1)} %bitcast.142), calls=%async_computation.3 | async-start | bytes 3145728 | tf_op jit(solution)/shard_map/all_to_all | solution.py:147
  204.8 0.0 copy-done.4
  204.8 25.8 %reduce-scatter.3.cloned.1.call-done = bf16[64,2,2048]{2,0,1:T(8,128)(2,1)} async-done(((bf16[256,2,2048]{2,0,1:T(8,128)(2,1)}), bf16[64,2,2048]{2,0,1:T(8,128)(2,1)}) %reduce-scatter.3.cloned.1.call-update) | async-done | bytes 524304 | tf_op jit(solution)/shard_map/reduce_scatter | solution.py:102
  230.6 2.4 copy.55
  232.9 0.0 all-to-all-done.1
  232.9 0.5 convolution_multiply_fusion.2
  233.4 1.3 fusion.26
  (35 shorter events, 0.4 us)
Async XLA Ops:
  7.2 100.8 %copy-start = (bf16[1,256,2048]{2,1,0:T(8,128)(2,1)S(1)}, bf16[1,256,2048]{2,1,0:T(8,128)(2,1)}, u32[]{:S(2)}) copy-start(bf16[1,256,2048]{2,1,0:T(8,128)(2,1)} %param.27) | copy-start | bytes 3145732
  7.2 95.0 %copy-start.7 = (bf16[1,2048,256]{2,1,0:T(8,128)(2,1)S(1)}, bf16[1,2048,256]{2,1,0:T(8,128)(2,1)}, u32[]{:S(2)}) copy-start(bf16[1,2048,256]{2,1,0:T(8,128)(2,1)} %param.25) | copy-start | bytes 3145732
  7.2 95.0 %all-gather.3.cloned.1.call-start = ((), (), s32[]{:S(2)}) async-start(), calls=%async_computation.5 | async-start | bytes 7864320 | tf_op jit(solution)/shard_map/all_gather | solution.py:136
  56.6 51.4 %copy-start.8 = (bf16[1,2048,256]{2,1,0:T(8,128)(2,1)S(1)}, bf16[1,2048,256]{2,1,0:T(8,128)(2,1)}, u32[]{:S(2)}) copy-start(bf16[1,2048,256]{2,1,0:T(8,128)(2,1)} %param.26) | copy-start | bytes 3145732
  56.7 142.5 %reduce-scatter.5.cloned.1.call-start = ((), (), s32[]{:S(2)}) async-start(), calls=%async_computation.6 | async-start | bytes 7864320 | tf_op jit(solution)/shard_map/reduce_scatter | solution.py:141
  120.3 0.7 copy-start.6
  120.3 1.0 copy-start.2
  120.3 1.4 copy-start.1
  120.3 1.4 copy-start.5
  120.3 33.1 %copy-start.3 = (bf16[256,2,64]{0,2,1:T(8,128)(2,1)S(1)}, bf16[256,2,64]{0,2,1:T(8,128)(2,1)}, u32[]{:S(2)}) copy-start(bf16[256,2,64]{0,2,1:T(8,128)(2,1)} %param.17) | copy-start | bytes 196612
  120.3 110.2 %reduce-scatter.3.cloned.1.call-start = ((), (), s32[]{:S(2)}) async-start(), calls=%async_computation.4 | async-start | bytes 2621440 | tf_op jit(solution)/shard_map/reduce_scatter | solution.py:102
  195.7 9.0 %copy-start.4 = (f32[128,2]{0,1:T(2,128)S(1)}, f32[128,2]{0,1:T(2,128)}, u32[]{:S(2)}) copy-start(f32[128,2]{0,1:T(2,128)} %param.24) | copy-start | bytes 3076
  199.1 33.8 %all-to-all-start.1 = ((bf16[8,48,2048]{2,1,0:T(8,128)(2,1)}), bf16[8,48,2048]{2,1,0:T(8,128)(2,1)S(1)}, u32[]{:S(2)}, u32[]{:S(2)}) async-start(bf16[8,48,2048]{2,1,0:T(8,128)(2,1)} %bitcast.142), calls=%async_computation.3 | async-start | bytes 3145728 | tf_op jit(solution)/shard_map/all_to_all | solution.py:147
Sparse Core Ops, SparseCore 0:
  56.8 45.3 all-gather.2
  120.5 58.8 reduce-scatter.4
  199.2 31.3 reduce-scatter.2
where the time goes:
time: 242 us; the launch traced here: 241 us
  blocking collectives  107 us (44%)
  waiting for transfers between devices  71.3 us (29%)
  matrix products  31.9 us (13%)
  between operations  14 us (6%)
  other arithmetic  5.82 us (2%)
  starting transfers between devices  5.78 us (2%)
  local copies, waits for them, and re-layouts  5.07 us (2%)
    all_gather x1, waiting for transfers between devices, per_device(): rows = lax.all_gather(received, 'tp', axis=0, tiled=True)  45.5 us
    all_to_all x1, blocking collectives, per_device(): lax.all_to_all(send, 'ep', split_axis=0, concat_axis=0, tiled=True)  44.2 us
    all_gather x1, blocking collectives, per_device(): value_piece = lax.all_gather(value_heads, 'ep', axis=0, tiled=True)  31.5 us
    all_gather x1, blocking collectives, per_device(): key_piece = lax.all_gather(k_rot, 'ep', axis=0, tiled=True)  31.5 us
    reduce_scatter x1, waiting for transfers between devices, per_device(): lax.psum_scatter(product.reshape(pos_count // lax.axis_size('tp') * lax.a...  25.8 us
    dot_general x1, matrix products, per_device(): jnp.dot(rows, w_down[0], preferred_element_type=jnp.float32)  12.3 us
    dot_general x1, matrix products, per_device(): gate = jnp.dot(rows, w_gate[0], preferred_element_type=jnp.float32)  5.8 us
    all_to_all x1, starting transfers between devices, per_device(): lax.all_to_all(result, 'ep', split_axis=0, concat_axis=0, tiled=True)  5.66 us
  transfers between devices with their start and end apart: 4, of which 2 were waited for; matrix products, arithmetic and copies ran while one was open for 7% of the time, Pallas kernels for 0%

commit v1 on v0

--- a/solution.py
+++ b/solution.py
@@ -63,7 +63,13 @@
     )
     carry = start_state
     key_piece = lax.all_gather(k_rot, "ep", axis=0, tiled=True)
-    value_piece = lax.all_gather(value_heads, "ep", axis=0, tiled=True)
+    size = lax.axis_size("ep")
+    held, blocks = (value_heads, [value_heads])
+    for _ in range(size - 1):
+        held = lax.ppermute(held, "ep", [(i, (i + 1) % size) for i in range(size)])
+        blocks.insert(0, held)
+    merged = jnp.concatenate(blocks, axis=0)
+    value_piece = jnp.roll(merged, (lax.axis_index("ep") + 1) * value_heads.shape[0], axis=0)
     count = key_piece.shape[0]
     width = math.gcd(count, 512)
     key_split = key_piece.reshape(count // width, width, seq_count, kv_local, HEAD_DIM)

time: 242 us -> 249 us (1.029)
  waiting for transfers between devices: 71.3 us -> 108 us
  blocking collectives: 107 us -> 75.8 us
    ppermute x0 -> x7, waiting for transfers between devices: none -> 37.7 us  [per_device(): held = lax.ppermute(held, 'ep', [(i, (i + 1) % size) for i in range(size)])]
    all_gather x1 -> x0, blocking collectives: 31.5 us -> none  [per_device(): value_piece = lax.all_gather(value_heads, 'ep', axis=0, tiled=True)]
    ppermute x0 -> x7, starting transfers between devices: none -> 3.55 us  [per_device(): held = lax.ppermute(held, 'ep', [(i, (i + 1) % size) for i in range(size)])]
  transfers between devices with their start and end apart: 4 -> 11, of which waited for: 2 -> 8; matrix products, arithmetic and copies ran while one was open for 7% -> 7% of each run, Pallas kernels for 0% -> 0%
where the time goes in v1:
time: 249 us; the launch traced here: 248 us
  waiting for transfers between devices  108 us (43%)
  blocking collectives  75.8 us (30%)
  matrix products  31.9 us (13%)
  between operations  14.1 us (6%)
  starting transfers between devices  7.27 us (3%)
  other arithmetic  5.81 us (2%)
  local copies, waits for them, and re-layouts  4.8 us (2%)
    all_gather x1, waiting for transfers between devices, per_device(): rows = lax.all_gather(received, 'tp', axis=0, tiled=True)  45.5 us
    all_to_all x1, blocking collectives, per_device(): lax.all_to_all(send, 'ep', split_axis=0, concat_axis=0, tiled=True)  44.2 us
    ppermute x7, waiting for transfers between devices, per_device(): held = lax.ppermute(held, 'ep', [(i, (i + 1) % size) for i in range(size)])  37.7 us
    all_gather x1, blocking collectives, per_device(): key_piece = lax.all_gather(k_rot, 'ep', axis=0, tiled=True)  31.6 us
    reduce_scatter x1, waiting for transfers between devices, per_device(): lax.psum_scatter(product.reshape(pos_count // lax.axis_size('tp') * lax.a...  25.2 us
    dot_general x1, matrix products, per_device(): jnp.dot(rows, w_down[0], preferred_element_type=jnp.float32)  12.3 us
    dot_general x1, matrix products, per_device(): gate = jnp.dot(rows, w_gate[0], preferred_element_type=jnp.float32)  5.76 us
  transfers between devices with their start and end apart: 11, of which 8 were waited for; matrix products, arithmetic and copies ran while one was open for 7% of the time, Pallas kernels for 0%

profile of v1, /device:TPU:0, one launch (start us, length us, event | category | flops | bytes accessed | tf_op | source)
XLA Modules:
  0.0 248.3 jit_solution(2624585522900132535)
XLA Ops:
  7.2 0.0 copy-start
  7.2 0.0 all-gather.2.cloned.1.call-start
  7.2 1.4 fusion.28
  8.6 0.8 copy.53
  9.4 0.1 eq.66
  9.5 0.2 fusion.27
  9.8 0.1 convert_element_type.99
  9.9 0.1 copy.54
  10.0 0.7 multiply_add_fusion
  10.7 0.1 convert_reduce_fusion
  10.7 1.7 convolution_convert_fusion.2
  12.4 44.2 %all_to_all.24 = bf16[8,48,2048]{2,1,0:T(8,128)(2,1)} all-to-all(bf16[8,48,2048]{2,1,0:T(8,128)(2,1)S(1)} %bitcast.141), channel_id=1, replica_groups=mesh['ep'=8,'tp'=4] {'ep'}, dimensions={0} | all-to-all | bytes 3145728 | tf_op jit(solution)/shard_map/all_to_all | solution.py:141
  56.6 0.0 all-gather.2.cloned.1.call-update
  56.6 0.0 copy-start.8
  56.7 0.0 reduce-scatter.5.cloned.1.call-start
  56.7 45.5 %all-gather.2.cloned.1.call-done = bf16[1536,2048]{1,0:T(8,128)(2,1)} async-done(((bf16[384,2048]{1,0:T(8,128)(2,1)}), bf16[1536,2048]{1,0:T(8,128)(2,1)}) %all-gather.2.cloned.1.call-update) | async-done | bytes 6291472 | tf_op jit(solution)/shard_map/all_gather | solution.py:142
  102.2 5.8 %fusion.34 = f32[1536,256]{1,0:T(8,128)} fusion(bf16[1536,2048]{1,0:T(8,128)(2,1)} %all-gather.2.cloned.1.call-done, bf16[1,2048,256]{2,1,0:T(8,128)(2,1)S(1)} %copy-done.7), kind=kOutput, calls=%fused_computation.44 | convolution fusion | flops 1610612736 | bytes 8912896 | tf_op jit(solution)/shard_map/dot_general | solution.py:143
  108.0 12.3 %convolution_convert_fusion = bf16[1536,2048]{1,0:T(8,128)(2,1)} fusion(bf16[1536,2048]{1,0:T(8,128)(2,1)} %all-gather.2.cloned.1.call-done, f32[1536,256]{1,0:T(8,128)} %fusion.34, bf16[1,256,2048]{2,1,0:T(8,128)(2,1)S(1)} %copy-done, bf16[1,2048,256]{2,1,0:T(8,128)(2,1)S(1)} %copy-done.8), kind=kOutput, calls=%fused_computation.26 | convolution fusion | flops 3226730496 | bytes 16252928 | tf_op jit(solution)/shard_map/dot_general | solution.py:148
  120.3 0.0 copy-start.5
  120.3 0.0 reduce-scatter.5.cloned.1.call-update
  120.3 0.0 reduce-scatter.3.cloned.1.call-start
  120.4 0.7 copy-done.3
  121.1 1.5 collective-permute-start
  122.6 0.1 mul.278
  122.7 0.2 copy.49
  122.9 0.1 broadcast_multiply_fusion.1
  123.0 0.1 fusion.47
  123.1 0.1 bitcast_reduce_fusion.1
  123.2 0.1 multiply_multiply_fusion
  123.3 0.1 subtract_convert_fusion
  123.4 4.6 %collective-permute-done = bf16[256,2,1,64]{0,3,1,2:T(8,128)(2,1)S(1)} collective-permute-done((bf16[256,2,1,64]{0,3,1,2:T(8,128)(2,1)S(1)}, bf16[256,2,1,64]{0,3,1,2:T(8,128)(2,1)S(1)}, u32[]{:S(2)}, u32[]{:S(2)}) %collective-permute-start) | collective-permute-done | bytes 65568 | tf_op jit(solution)/shard_map/ppermute | solution.py:69
  128.1 7.0 %collective-permute-done.1 = bf16[256,2,1,64]{0,3,1,2:T(8,128)(2,1)S(1)} collective-permute-done((bf16[256,2,1,64]{0,3,1,2:T(8,128)(2,1)S(1)}, bf16[256,2,1,64]{0,3,1,2:T(8,128)(2,1)S(1)}, u32[]{:S(2)}, u32[]{:S(2)}) %collective-permute-start.1) | collective-permute-done | bytes 65568 | tf_op jit(solution)/shard_map/ppermute | solution.py:69
  135.0 0.1 fusion.42
  135.1 6.9 %collective-permute-done.2 = bf16[256,2,1,64]{0,3,1,2:T(8,128)(2,1)S(1)} collective-permute-done((bf16[256,2,1,64]{0,3,1,2:T(8,128)(2,1)S(1)}, bf16[256,2,1,64]{0,3,1,2:T(8,128)(2,1)S(1)}, u32[]{:S(2)}, u32[]{:S(2)}) %collective-permute-start.2) | collective-permute-done | bytes 65568 | tf_op jit(solution)/shard_map/ppermute | solution.py:69
  142.0 6.9 %collective-permute-done.3 = bf16[256,2,1,64]{0,3,1,2:T(8,128)(2,1)S(1)} collective-permute-done((bf16[256,2,1,64]{0,3,1,2:T(8,128)(2,1)S(1)}, bf16[256,2,1,64]{0,3,1,2:T(8,128)(2,1)S(1)}, u32[]{:S(2)}, u32[]{:S(2)}) %collective-permute-start.3) | collective-permute-done | bytes 65568 | tf_op jit(solution)/shard_map/ppermute | solution.py:69
  149.0 0.0 collective-permute-start.4
  149.0 7.2 %collective-permute-done.4 = bf16[256,2,1,64]{0,3,1,2:T(8,128)(2,1)S(1)} collective-permute-done((bf16[256,2,1,64]{0,3,1,2:T(8,128)(2,1)S(1)}, bf16[256,2,1,64]{0,3,1,2:T(8,128)(2,1)S(1)}, u32[]{:S(2)}, u32[]{:S(2)}) %collective-permute-start.4) | collective-permute-done | bytes 65568 | tf_op jit(solution)/shard_map/ppermute | solution.py:69
  156.1 31.6 %all_gather.6 = bf16[2048,2,1,64]{0,3,1,2:T(8,128)(2,1)S(1)} all-gather(bf16[256,2,1,64]{0,3,1,2:T(8,128)(2,1)S(1)} %bitcast.153), channel_id=1, replica_groups=mesh['ep'=8,'tp'=4] {'ep'}, dimensions={0}, use_global_device_ids=true | all-gather | bytes 589824 | tf_op jit(solution)/shard_map/all_gather | solution.py:65
  187.8 0.0 collective-permute-done.5
  187.8 2.1 collective-permute-start.6
  189.9 5.1 %collective-permute-done.6 = bf16[256,2,1,64]{0,3,1,2:T(8,128)(2,1)S(1)} collective-permute-done((bf16[256,2,1,64]{0,3,1,2:T(8,128)(2,1)S(1)}, bf16[256,2,1,64]{0,3,1,2:T(8,128)(2,1)S(1)}, u32[]{:S(2)}, u32[]{:S(2)}) %collective-permute-start.6) | collective-permute-done | bytes 65568 | tf_op jit(solution)/shard_map/ppermute | solution.py:69
  195.2 0.1 constant_dynamic-slice_fusion
  195.3 10.0 %while.15 = (s32[]{:T(128)}, f32[2,1,4,256]{3,2,0,1:T(4,128)S(1)}, f32[2,1,4,256]{3,2,0,1:T(4,128)S(1)}, f32[256,2,1,4,64]{0,4,3,1,2:T(8,128)S(1)}, bf16[4,512,2...) while((s32[]{:T(128)}, f32[2,1,4,256]{3,2,0,1:T(4,128)S(1)}, ...), condition=%wide.region_5.6_spmd.clone, body=%wide.region_2.5_spmd.clone.sunk | while | flops 277229568 | bytes 14286969 | solution.py:98
  195.3 0.8 bitcast_reduce_fusion.3
  196.1 0.7 fusion.67
  196.8 0.9 fusion.68
  197.8 0.8 bitcast_reduce_fusion.3
  198.6 0.7 fusion.67
  199.3 0.9 fusion.68
  200.3 0.8 bitcast_reduce_fusion.3
  201.1 0.7 fusion.67
  201.8 0.9 fusion.68
  202.8 0.8 bitcast_reduce_fusion.3
  203.6 0.7 fusion.67
  204.3 1.0 fusion.68
  205.4 0.0 copy-start.4
  205.4 3.3 %convolution_convert_fusion.1 = bf16[256,2,2048]{2,0,1:T(8,128)(2,1)} fusion(bf16[256,2,256]{0,2,1:T(8,128)(2,1)S(1)} %bitcast.150, bf16[256,2048]{1,0:T(8,128)(2,1)} %param.20), kind=kOutput, calls=%fused_computation.27 | convolution fusion | flops 537919488 | bytes 3407872 | tf_op jit(solution)/shard_map/dot_general | solution.py:103
  208.7 0.0 reduce-scatter.3.cloned.1.call-update
  208.7 0.0 reduce-scatter.5.cloned.1.call-done
  208.8 3.6 %all-to-all-start.1 = ((bf16[8,48,2048]{2,1,0:T(8,128)(2,1)}), bf16[8,48,2048]{2,1,0:T(8,128)(2,1)S(1)}, u32[]{:S(2)}, u32[]{:S(2)}) async-start(bf16[8,48,2048]{2,1,0:T(8,128)(2,1)} %bitcast.149), calls=%async_computation.3 | async-start | bytes 3145728 | tf_op jit(solution)/shard_map/all_to_all | solution.py:153
  212.4 25.2 %reduce-scatter.3.cloned.1.call-done = bf16[64,2,2048]{2,0,1:T(8,128)(2,1)} async-done(((bf16[256,2,2048]{2,0,1:T(8,128)(2,1)}), bf16[64,2,2048]{2,0,1:T(8,128)(2,1)}) %reduce-scatter.3.cloned.1.call-update) | async-done | bytes 524304 | tf_op jit(solution)/shard_map/reduce_scatter | solution.py:108
  237.6 2.4 copy.55
  240.0 0.5 convolution_multiply_fusion.2
  240.5 1.3 fusion.26
  (64 shorter events, 0.6 us)
Async XLA Ops:
  7.2 100.8 %copy-start = (bf16[1,256,2048]{2,1,0:T(8,128)(2,1)S(1)}, bf16[1,256,2048]{2,1,0:T(8,128)(2,1)}, u32[]{:S(2)}) copy-start(bf16[1,256,2048]{2,1,0:T(8,128)(2,1)} %param.27) | copy-start | bytes 3145732
  7.2 95.0 %copy-start.7 = (bf16[1,2048,256]{2,1,0:T(8,128)(2,1)S(1)}, bf16[1,2048,256]{2,1,0:T(8,128)(2,1)}, u32[]{:S(2)}) copy-start(bf16[1,2048,256]{2,1,0:T(8,128)(2,1)} %param.25) | copy-start | bytes 3145732
  7.2 95.0 %all-gather.2.cloned.1.call-start = ((), (), s32[]{:S(2)}) async-start(), calls=%async_computation.5 | async-start | bytes 7864320 | tf_op jit(solution)/shard_map/all_gather | solution.py:142
  56.6 51.3 %copy-start.8 = (bf16[1,2048,256]{2,1,0:T(8,128)(2,1)S(1)}, bf16[1,2048,256]{2,1,0:T(8,128)(2,1)}, u32[]{:S(2)}) copy-start(bf16[1,2048,256]{2,1,0:T(8,128)(2,1)} %param.26) | copy-start | bytes 3145732
  56.7 152.1 %reduce-scatter.5.cloned.1.call-start = ((), (), s32[]{:S(2)}) async-start(), calls=%async_computation.6 | async-start | bytes 7864320 | tf_op jit(solution)/shard_map/reduce_scatter | solution.py:147
  120.3 0.8 copy-start.3
  120.3 2.3 copy-start.6
  120.3 2.4 copy-start.2
  120.3 3.1 %copy-start.1 = (bf16[256,2,64]{0,2,1:T(8,128)(2,1)S(1)}, bf16[256,2,64]{0,2,1:T(8,128)(2,1)}, u32[]{:S(2)}) copy-start(bf16[256,2,64]{0,2,1:T(8,128)(2,1)} %param.16) | copy-start | bytes 196612
  120.3 14.8 %copy-start.5 = (f32[64]{0:T(128)S(1)}, f32[64]{0:T(128)}, u32[]{:S(2)}) copy-start(f32[64]{0:T(128)} %param.19) | copy-start | bytes 772
  120.3 117.3 %reduce-scatter.3.cloned.1.call-start = ((), (), s32[]{:S(2)}) async-start(), calls=%async_computation.4 | async-start | bytes 2621440 | tf_op jit(solution)/shard_map/reduce_scatter | solution.py:108
  121.1 7.0 %collective-permute-start = (bf16[256,2,1,64]{0,3,1,2:T(8,128)(2,1)S(1)}, bf16[256,2,1,64]{0,3,1,2:T(8,128)(2,1)S(1)}, u32[]{:S(2)}, u32[]{:S(2)}) collective-permute-start(bf16[256,2,1,64]{0,3,1,2:T(8,128)(2,1)S(1)} %bitcast.154), channel_id=1, source_target_pairs={{0,4},{4,8},{8,12},{12,16},{16,20},{20,24},{24,28},{28,0},{1,5},{5... | collective-permute-start | bytes 196616 | tf_op jit(solution)/shard_map/ppermute | solution.py:69
  128.1 7.0 %collective-permute-start.1 = (bf16[256,2,1,64]{0,3,1,2:T(8,128)(2,1)S(1)}, bf16[256,2,1,64]{0,3,1,2:T(8,128)(2,1)S(1)}, u32[]{:S(2)}, u32[]{:S(2)}) collective-permute-start(bf16[256,2,1,64]{0,3,1,2:T(8,128)(2,1)S(1)} %collective-permute-done), channel_id=1, source_target_pairs={{0,4},{4,8},{8,12},{12,16},{16,20},{20,24},{24,28},{28,0},{1,5},{5... | collective-permute-start | bytes 196616 | tf_op jit(solution)/shard_map/ppermute | solution.py:69
  135.0 7.0 %collective-permute-start.2 = (bf16[256,2,1,64]{0,3,1,2:T(8,128)(2,1)S(1)}, bf16[256,2,1,64]{0,3,1,2:T(8,128)(2,1)S(1)}, u32[]{:S(2)}, u32[]{:S(2)}) collective-permute-start(bf16[256,2,1,64]{0,3,1,2:T(8,128)(2,1)S(1)} %collective-permute-done.1), channel_id=1, source_target_pairs={{0,4},{4,8},{8,12},{12,16},{16,20},{20,24},{24,28},{28,0},{1,5},{5... | collective-permute-start | bytes 196616 | tf_op jit(solution)/shard_map/ppermute | solution.py:69
  142.0 7.0 %collective-permute-start.3 = (bf16[256,2,1,64]{0,3,1,2:T(8,128)(2,1)S(1)}, bf16[256,2,1,64]{0,3,1,2:T(8,128)(2,1)S(1)}, u32[]{:S(2)}, u32[]{:S(2)}) collective-permute-start(bf16[256,2,1,64]{0,3,1,2:T(8,128)(2,1)S(1)} %collective-permute-done.2), channel_id=1, source_target_pairs={{0,4},{4,8},{8,12},{12,16},{16,20},{20,24},{24,28},{28,0},{1,5},{5... | collective-permute-start | bytes 196616 | tf_op jit(solution)/shard_map/ppermute | solution.py:69
  149.0 7.2 %collective-permute-start.4 = (bf16[256,2,1,64]{0,3,1,2:T(8,128)(2,1)S(1)}, bf16[256,2,1,64]{0,3,1,2:T(8,128)(2,1)S(1)}, u32[]{:S(2)}, u32[]{:S(2)}) collective-permute-start(bf16[256,2,1,64]{0,3,1,2:T(8,128)(2,1)S(1)} %collective-permute-done.3), channel_id=1, source_target_pairs={{0,4},{4,8},{8,12},{12,16},{16,20},{20,24},{24,28},{28,0},{1,5},{5... | collective-permute-start | bytes 196616 | tf_op jit(solution)/shard_map/ppermute | solution.py:69
  156.1 31.6 %collective-permute-start.5 = (bf16[256,2,1,64]{0,3,1,2:T(8,128)(2,1)S(1)}, bf16[256,2,1,64]{0,3,1,2:T(8,128)(2,1)S(1)}, u32[]{:S(2)}, u32[]{:S(2)}) collective-permute-start(bf16[256,2,1,64]{0,3,1,2:T(8,128)(2,1)S(1)} %collective-permute-done.4), channel_id=1, source_target_pairs={{0,4},{4,8},{8,12},{12,16},{16,20},{20,24},{24,28},{28,0},{1,5},{5... | collective-permute-start | bytes 196616 | tf_op jit(solution)/shard_map/ppermute | solution.py:69
  187.8 7.2 %collective-permute-start.6 = (bf16[256,2,1,64]{0,3,1,2:T(8,128)(2,1)S(1)}, bf16[256,2,1,64]{0,3,1,2:T(8,128)(2,1)S(1)}, u32[]{:S(2)}, u32[]{:S(2)}) collective-permute-start(bf16[256,2,1,64]{0,3,1,2:T(8,128)(2,1)S(1)} %collective-permute-done.5), channel_id=1, source_target_pairs={{0,4},{4,8},{8,12},{12,16},{16,20},{20,24},{24,28},{28,0},{1,5},{5... | collective-permute-start | bytes 196616 | tf_op jit(solution)/shard_map/ppermute | solution.py:69
  205.4 7.0 %copy-start.4 = (f32[128,2]{0,1:T(2,128)S(1)}, f32[128,2]{0,1:T(2,128)}, u32[]{:S(2)}) copy-start(f32[128,2]{0,1:T(2,128)} %param.24) | copy-start | bytes 3076
  208.8 31.2 %all-to-all-start.1 = ((bf16[8,48,2048]{2,1,0:T(8,128)(2,1)}), bf16[8,48,2048]{2,1,0:T(8,128)(2,1)S(1)}, u32[]{:S(2)}, u32[]{:S(2)}) async-start(bf16[8,48,2048]{2,1,0:T(8,128)(2,1)} %bitcast.149), calls=%async_computation.3 | async-start | bytes 3145728 | tf_op jit(solution)/shard_map/all_to_all | solution.py:153
Sparse Core Ops, SparseCore 0:
  56.8 45.3 all-gather.1
  120.4 58.8 reduce-scatter.4
  208.9 28.7 reduce-scatter.2
